TPU v7x, 256 devices: a whole 4x4x8 slice. The times are simulated.
256 devices in a mesh: ep: 16 (over y, x), tp: 16 (over z, core).
Axes of the slice: x: 4, y: 4, z: 8, core: 2. Of those that a mesh axis runs over, the one named last changes fastest.
Arguments:
- mix_tokens: bfloat16 [32768, 2048], P(('ep', 'tp')), may hold values from -6 to 6
- mix_gain: bfloat16 [2048], replicated, may hold values from 0.099609375 to 1.8984375
- gate_proj: bfloat16 [2048, 1024], P(None, 'tp'), may hold values from -0.125 to 0.125
- conv_proj: bfloat16 [2048, 1024], P(None, 'tp'), may hold values from -0.125 to 0.125
- value_proj: bfloat16 [2048, 1024], P(None, 'tp'), may hold values from -0.125 to 0.125
- conv_taps: bfloat16 [3, 1024], P(None, 'tp'), may hold values from -3 to 3
- out_proj: bfloat16 [1024, 2048], P('tp'), may hold values from -0.1875 to 0.1875
- moe_tokens: bfloat16 [16384, 2048], P(('ep', 'tp')), may hold values from -6 to 6
- moe_gain: bfloat16 [2048], replicated, may hold values from 0.099609375 to 1.8984375
- expert_ids: int32 [16384, 2], P(('ep', 'tp')), may hold values from 0 to 15, all different within a row; in each aligned block of 64 rows (0 to 63, 64 to 127, ...) at most 9 rows name the same one
- expert_scores: float32 [16384, 2], P(('ep', 'tp')), may hold values from -6 to 6
- expert_gate: bfloat16 [16, 2048, 4096], P('ep', None, 'tp'), may hold values from -0.125 to 0.125
- expert_up: bfloat16 [16, 2048, 4096], P('ep', None, 'tp'), may hold values from -0.125 to 0.125
- expert_down: bfloat16 [16, 4096, 2048], P('ep', 'tp'), may hold values from -0.09375 to 0.09375
Outputs:
- mix_out: bfloat16 [32768, 2048], P(('ep', 'tp'))
- moe_out: bfloat16 [16384, 2048], P(('ep', 'tp'))
Inputs may be any that keep to these rules, and one draw needn't show every extreme that they name: `expert_ids`: each row names 2 different experts; among the rows of one device no expert is named more than 9 times.
All inputs are finite; a program needn't handle non-finite values.
Results may differ from a plain program's by a relative error of at most 0.018.
Values may be sent and summed in bfloat16 or wider, within the bound.
A program may use at most 128 MiB of HBM per device.

v0:
```python
import jax
import jax.numpy as jnp
from jax import lax
from jax.sharding import PartitionSpec as P

norm_eps = 1e-06


def from_behind(value, axis, steps):
    count = lax.axis_size(axis)
    leading, last = (max(0, -steps), min(count, count - steps))
    return lax.ppermute(value, axis, [(source, source + steps) for source in range(leading, last)])


def scaled_norm(row_data, gain_vec):
    values = row_data.astype(jnp.float32)
    inverse = lax.rsqrt(jnp.mean(values * values, axis=1, keepdims=True) + norm_eps)
    return (values * inverse * gain_vec.astype(jnp.float32)).astype(jnp.bfloat16)


def shards(
    mix_tokens,
    mix_gain,
    gate_proj,
    conv_proj,
    value_proj,
    conv_taps,
    out_proj,
    moe_tokens,
    moe_gain,
    expert_ids,
    expert_scores,
    expert_gate,
    expert_up,
    expert_down,
):
    normed = scaled_norm(mix_tokens, mix_gain)
    w_joint = jnp.concatenate([gate_proj, conv_proj, value_proj], axis=1)
    combined = jnp.dot(
        lax.all_gather(normed, "tp", axis=0, tiled=True),
        w_joint,
        preferred_element_type=jnp.float32,
    ).astype(jnp.bfloat16)
    channels = gate_proj.shape[1]
    out_gate = combined[:, :channels]
    in_gate = combined[:, channels : 2 * channels]
    values = combined[:, 2 * channels :]
    signal = (in_gate.astype(jnp.float32) * values.astype(jnp.float32)).astype(jnp.bfloat16)
    tap_count = conv_taps.shape[0]
    before = from_behind(signal[signal.shape[0] - (tap_count - 1) :], "ep", 1)
    extended = jnp.concatenate([before, signal], axis=0)
    length = signal.shape[0]
    tap_values = conv_taps.astype(jnp.float32)
    convolved = jnp.zeros((length, channels), jnp.float32)
    for offset in range(tap_count):
        convolved = (
            convolved + extended[offset : offset + length].astype(jnp.float32) * tap_values[offset]
        )
    carried = (out_gate.astype(jnp.float32) * convolved).astype(jnp.bfloat16)
    token_major = lax.all_to_all(carried, "tp", split_axis=0, concat_axis=1, tiled=True)
    mix_out = jnp.dot(
        token_major,
        lax.all_gather(out_proj, "tp", axis=0, tiled=True),
        preferred_element_type=jnp.float32,
    ).astype(jnp.bfloat16)
    moe_normed = scaled_norm(moe_tokens, moe_gain)
    experts = expert_gate.shape[0] * lax.axis_size("ep")
    row_count, top_count = expert_ids.shape
    capacity = top_count * row_count // experts + max(1, top_count * row_count // (8 * experts))
    width_model = moe_tokens.shape[1]
    flat_ids = expert_ids.reshape(-1)
    onehot = (flat_ids[:, None] == jnp.arange(experts, dtype=jnp.int32)[None, :]).astype(jnp.int32)
    slot_rank = jnp.sum((jnp.cumsum(onehot, axis=0) - onehot) * onehot, axis=1)
    slot_index = flat_ids * capacity + slot_rank
    slot_match = slot_index[:, None] == jnp.arange(experts * capacity, dtype=jnp.int32)[None, :]
    dispatch_map = jnp.any(
        slot_match.reshape(row_count, top_count, experts * capacity), axis=1
    ).astype(jnp.bfloat16)
    outgoing = lax.dot_general(
        dispatch_map, moe_normed, (((0,), (0,)), ((), ())), preferred_element_type=jnp.float32
    ).astype(jnp.bfloat16)
    arrived = lax.all_to_all(
        outgoing.reshape(experts, capacity, width_model),
        "ep",
        split_axis=0,
        concat_axis=0,
        tiled=True,
    )
    arrived_rows = arrived.reshape(-1, width_model)
    w_gate = expert_gate[0]
    w_up = expert_up[0]
    w_down = expert_down[0]
    portion = lax.all_gather(arrived_rows, "tp", axis=0, tiled=True)
    gate_value = jnp.dot(portion, w_gate, preferred_element_type=jnp.float32)
    up_value = jnp.dot(portion, w_up, preferred_element_type=jnp.float32)
    hidden = (jax.nn.silu(gate_value) * up_value).astype(jnp.bfloat16)
    summed = lax.psum_scatter(
        jnp.dot(hidden, w_down, preferred_element_type=jnp.float32).astype(jnp.bfloat16),
        "tp",
        scatter_dimension=0,
        tiled=True,
    )
    returned = lax.all_to_all(
        summed.reshape(experts, capacity, width_model),
        "ep",
        split_axis=0,
        concat_axis=0,
        tiled=True,
    )
    flat_back = returned.reshape(experts * capacity, width_model)
    picked = flat_back[slot_index].reshape(row_count, top_count, width_model)
    route_weight = jax.nn.softmax(expert_scores, axis=1)
    moe_out = jnp.sum(route_weight[:, :, None] * picked.astype(jnp.float32), axis=1).astype(
        jnp.bfloat16
    )
    return (mix_out, moe_out)


def solution(mesh):
    in_specs = (
        P(("ep", "tp"), None),
        P(),
        P(None, "tp"),
        P(None, "tp"),
        P(None, "tp"),
        P(None, "tp"),
        P("tp", None),
        P(("ep", "tp"), None),
        P(),
        P(("ep", "tp"), None),
        P(("ep", "tp"), None),
        P("ep", None, "tp"),
        P("ep", None, "tp"),
        P("ep", "tp", None),
    )
    out_specs = (P(("ep", "tp"), None), P(("ep", "tp"), None))
    return jax.shard_map(shards, mesh=mesh, in_specs=in_specs, out_specs=out_specs, check_vma=False)
```

profile of v0, /device:TPU:1, one launch (start us, length us, event | category | flops | bytes accessed | tf_op | source)
XLA Modules:
  0.0 292.0 jit_solution(8549273080741177627)
XLA Ops:
  7.2 0.0 copy-start
  7.2 0.0 all-gather.8.cloned.1.call-start
  7.2 0.8 copy.25
  8.1 0.1 eq.29
  8.2 0.1 fusion.24
  8.3 0.2 reduce_window_sum.11
  8.5 0.2 select_reduce_fusion
  8.7 0.1 reduce_sum.52
  8.8 0.1 copy.27
  8.9 0.1 fusion.23
  9.0 0.7 convert_element_type.89
  9.7 1.1 fusion.15
  10.8 1.3 convolution_convert_fusion.2
  12.2 0.2 reshape.87
  12.4 23.4 %all_to_all.29 = bf16[16,9,2048]{2,1,0:T(8,128)(2,1)S(1)} all-to-all(bf16[16,9,2048]{2,1,0:T(8,128)(2,1)S(1)} %reshape.87), channel_id=1, replica_groups=mesh['ep'=16,'tp'=16] {'ep'}, dimensions={0} | all-to-all | bytes 1179648 | tf_op jit(solution)/shard_map/all_to_all | solution.py:82
  35.8 1.1 reshape.88
  36.9 0.0 all-gather.8.cloned.1.call-update
  36.9 0.0 all-gather.4.cloned.1.call-start
  37.0 0.2 fusion.2
  37.2 1.0 fusion.4
  38.2 0.0 all-gather.4.cloned.1.call-update
  38.2 0.0 reduce-scatter.2.cloned.1.call-start
  38.3 60.5 %all-gather.8.cloned.1.call-done = bf16[2304,2048]{1,0:T(8,128)(2,1)} async-done(((bf16[144,2048]{1,0:T(8,128)(2,1)}), bf16[2304,2048]{1,0:T(8,128)(2,1)}) %all-gather.8.cloned.1.call-update) | async-done | bytes 9437200 | tf_op jit(solution)/shard_map/all_gather | solution.py:93
  98.7 7.7 %fusion.8 = f32[2304,256]{1,0:T(8,128)} fusion(bf16[2304,2048]{1,0:T(8,128)(2,1)} %all-gather.8.cloned.1.call-done, bf16[1,2048,256]{2,1,0:T(8,128)(2,1)S(1)} %copy-done.5), kind=kOutput, calls=%fused_computation.15 | convolution fusion | flops 2415919104 | bytes 12845056 | tf_op jit(solution)/shard_map/dot_general | solution.py:94
  106.5 14.9 %convolution_convert_fusion = bf16[2304,2048]{1,0:T(8,128)(2,1)} fusion(bf16[2304,2048]{1,0:T(8,128)(2,1)} %all-gather.8.cloned.1.call-done, f32[2304,256]{1,0:T(8,128)} %fusion.8, bf16[1,256,2048]{2,1,0:T(8,128)(2,1)S(1)} %copy-done, bf16[1,2048,256]{2,1,0:T(8,128)(2,1)} %param.26), kind=kOutput, calls=%fused_computation.1 | convolution fusion | flops 4840095744 | bytes 23330816 | tf_op jit(solution)/shard_map/dot_general | solution.py:98
  121.4 0.0 reduce-scatter.2.cloned.1.call-update
  121.4 0.0 all-gather.6.cloned.1.call-start
  121.5 0.5 all-gather.6.cloned.1.call-update
  122.0 0.1 copy-done.4
  122.1 33.5 %all-gather.4.cloned.1.call-done = bf16[2048,2048]{1,0:T(8,128)(2,1)} async-done(((bf16[128,2048]{1,0:T(8,128)(2,1)}), bf16[2048,2048]{1,0:T(8,128)(2,1)}) %all-gather.4.cloned.1.call-update) | async-done | bytes 8388624 | tf_op jit(solution)/shard_map/all_gather | solution.py:40
  155.6 6.3 %convolution_convert_fusion.1 = bf16[2048,192]{0,1:T(8,128)(2,1)S(1)} fusion(bf16[2048,2048]{1,0:T(8,128)(2,1)} %all-gather.4.cloned.1.call-done, bf16[2048,64]{0,1:T(8,128)(2,1)S(1)} %copy-done.6, bf16[2048,64]{0,1:T(8,128)(2,1)S(1)} %copy-done.7, bf16[2048,64]{0,1:T(8,128)(2,1)S(1)} %copy-done.8), kind=kOutput, calls=%fused_computation.4 | convolution fusion | flops 1613365248 | bytes 9961472 | tf_op jit(solution)/shard_map/dot_general | solution.py:39
  161.9 0.1 multiply_convert_fusion.1
  162.0 0.1 slice.41
  162.0 3.1 %collective-permute-start = (bf16[2,64]{0,1:T(8,128)(2,1)S(1)}, bf16[2,64]{0,1:T(8,128)(2,1)S(1)}, u32[]{:S(2)}, u32[]{:S(2)}) collective-permute-start(bf16[2,64]{0,1:T(8,128)(2,1)S(1)} %slice.41), channel_id=1, source_target_pairs={{0,16},{16,32},{32,48},{48,64},{64,80},{80,96},{96,112},{112,128},... | collective-permute-start | bytes 776 | tf_op jit(solution)/shard_map/ppermute | solution.py:12
  165.1 0.8 collective-permute-done
  166.0 1.0 copy_bitcast_fusion
  167.0 5.4 %all-to-all-start = ((bf16[16,128,64]{1,2,0:T(8,128)(2,1)}), bf16[16,128,64]{1,2,0:T(8,128)(2,1)S(1)}, u32[]{:S(2)}, u32[]{:S(2)}) async-start(bf16[16,128,64]{1,2,0:T(8,128)(2,1)} %copy_bitcast_fusion), calls=%async_computation | async-start | bytes 524288 | tf_op jit(solution)/shard_map/all_to_all | solution.py:60
  172.4 0.1 mul.138
  172.6 58.9 %reduce-scatter.2.cloned.1.call-done = bf16[144,2048]{1,0:T(8,128)(2,1)} async-done(((bf16[2304,2048]{1,0:T(8,128)(2,1)}), bf16[144,2048]{1,0:T(8,128)(2,1)}) %reduce-scatter.2.cloned.1.call-update) | async-done | bytes 589840 | tf_op jit(solution)/shard_map/reduce_scatter | solution.py:97
  231.5 2.3 reshape.89
  233.8 7.2 %all-to-all-start.2 = ((bf16[16,9,2048]{2,1,0:T(8,128)(2,1)}), bf16[16,9,2048]{2,1,0:T(8,128)(2,1)S(1)}, u32[]{:S(2)}, u32[]{:S(2)}) async-start(bf16[16,9,2048]{2,1,0:T(8,128)(2,1)} %reshape.89), calls=%async_computation.3 | async-start | bytes 2097152 | tf_op jit(solution)/shard_map/all_to_all | solution.py:103
  241.0 0.1 copy.24
  241.1 36.6 %all-gather.6.cloned.1.call-done = bf16[1024,2048]{1,0:T(8,128)(2,1)} async-done(((bf16[64,2048]{1,0:T(8,128)(2,1)}), bf16[1024,2048]{1,0:T(8,128)(2,1)}) %all-gather.6.cloned.1.call-update) | async-done | bytes 4194320 | tf_op jit(solution)/shard_map/all_gather | solution.py:63
  277.7 3.7 %convolution_convert_fusion.3 = bf16[128,2048]{1,0:T(8,128)(2,1)} fusion(bf16[128,1024]{0,1:T(8,128)(2,1)S(1)} %bitcast.36, bf16[1024,2048]{1,0:T(8,128)(2,1)} %all-gather.6.cloned.1.call-done), kind=kOutput, calls=%fused_computation.6 | convolution fusion | flops 537133056 | bytes 4980736 | tf_op jit(solution)/shard_map/dot_general | solution.py:61
  281.4 0.3 reshape.90
  281.6 0.9 gather_fusion
  282.6 0.7 reshape.91
  283.2 2.2 multiply_reduce_fusion
  (29 shorter events, 0.1 us)
Async XLA Ops:
  7.2 99.3 %copy-start = (bf16[1,256,2048]{2,1,0:T(8,128)(2,1)S(1)}, bf16[1,256,2048]{2,1,0:T(8,128)(2,1)}, u32[]{:S(2)}) copy-start(bf16[1,256,2048]{2,1,0:T(8,128)(2,1)} %param.27) | copy-start | bytes 3145732
  7.2 91.6 %all-gather.8.cloned.1.call-start = ((), (), s32[]{:S(2)}) async-start(), calls=%async_computation.6 | async-start | bytes 10027008 | tf_op jit(solution)/shard_map/all_gather | solution.py:93
  12.4 24.6 %copy-start.3 = (bf16[2048]{0:T(1024)(128)(2,1)S(1)}, bf16[2048]{0:T(1024)(128)(2,1)}, u32[]{:S(2)}) copy-start(bf16[2048]{0:T(1024)(128)(2,1)} %param.15) | copy-start | bytes 12292
  35.8 1.2 copy-start.1
  36.9 61.8 %copy-start.5 = (bf16[1,2048,256]{2,1,0:T(8,128)(2,1)S(1)}, bf16[1,2048,256]{2,1,0:T(8,128)(2,1)}, u32[]{:S(2)}) copy-start(bf16[1,2048,256]{2,1,0:T(8,128)(2,1)} %param.25) | copy-start | bytes 3145732
  36.9 118.6 %all-gather.4.cloned.1.call-start = ((), (), s32[]{:S(2)}) async-start(), calls=%async_computation.4 | async-start | bytes 8912896 | tf_op jit(solution)/shard_map/all_gather | solution.py:40
  38.2 193.3 %reduce-scatter.2.cloned.1.call-start = ((), (), s32[]{:S(2)}) async-start(), calls=%async_computation.7 | async-start | bytes 10027008 | tf_op jit(solution)/shard_map/reduce_scatter | solution.py:97
  121.4 0.7 copy-start.4
  121.4 34.2 %copy-start.6 = (bf16[2048,64]{0,1:T(8,128)(2,1)S(1)}, bf16[2048,64]{0,1:T(8,128)(2,1)}, u32[]{:S(2)}) copy-start(bf16[2048,64]{0,1:T(8,128)(2,1)} %param.18) | copy-start | bytes 786436
  121.4 34.2 %copy-start.7 = (bf16[2048,64]{0,1:T(8,128)(2,1)S(1)}, bf16[2048,64]{0,1:T(8,128)(2,1)}, u32[]{:S(2)}) copy-start(bf16[2048,64]{0,1:T(8,128)(2,1)} %param.17) | copy-start | bytes 786436
  121.4 34.2 %copy-start.8 = (bf16[2048,64]{0,1:T(8,128)(2,1)S(1)}, bf16[2048,64]{0,1:T(8,128)(2,1)}, u32[]{:S(2)}) copy-start(bf16[2048,64]{0,1:T(8,128)(2,1)} %param.16) | copy-start | bytes 786436
  121.4 156.2 %all-gather.6.cloned.1.call-start = ((), (), s32[]{:S(2)}) async-start(), calls=%async_computation.5 | async-start | bytes 4456448 | tf_op jit(solution)/shard_map/all_gather | solution.py:63
  122.1 50.5 %copy-start.2 = (f32[64,2]{0,1:T(2,128)S(1)}, f32[64,2]{0,1:T(2,128)}, u32[]{:S(2)}) copy-start(f32[64,2]{0,1:T(2,128)} %param.24) | copy-start | bytes 1540
  162.0 3.9 %collective-permute-start = (bf16[2,64]{0,1:T(8,128)(2,1)S(1)}, bf16[2,64]{0,1:T(8,128)(2,1)S(1)}, u32[]{:S(2)}, u32[]{:S(2)}) collective-permute-start(bf16[2,64]{0,1:T(8,128)(2,1)S(1)} %slice.41), channel_id=1, source_target_pairs={{0,16},{16,32},{32,48},{48,64},{64,80},{80,96},{96,112},{112,128},... | collective-permute-start | bytes 776 | tf_op jit(solution)/shard_map/ppermute | solution.py:12
  167.0 66.8 %all-to-all-start = ((bf16[16,128,64]{1,2,0:T(8,128)(2,1)}), bf16[16,128,64]{1,2,0:T(8,128)(2,1)S(1)}, u32[]{:S(2)}, u32[]{:S(2)}) async-start(bf16[16,128,64]{1,2,0:T(8,128)(2,1)} %copy_bitcast_fusion), calls=%async_computation | async-start | bytes 524288 | tf_op jit(solution)/shard_map/all_to_all | solution.py:60
  233.8 47.6 %all-to-all-start.2 = ((bf16[16,9,2048]{2,1,0:T(8,128)(2,1)}), bf16[16,9,2048]{2,1,0:T(8,128)(2,1)S(1)}, u32[]{:S(2)}, u32[]{:S(2)}) async-start(bf16[16,9,2048]{2,1,0:T(8,128)(2,1)} %reshape.89), calls=%async_computation.3 | async-start | bytes 2097152 | tf_op jit(solution)/shard_map/all_to_all | solution.py:103
Sparse Core Ops, SparseCore 0:
  37.0 61.6 all-gather.7
  101.1 54.3 all-gather.3
  158.1 73.3 reduce-scatter.1
  233.2 44.4 all-gather.5
where the time goes:
time: 293 us; the launch traced here: 292 us
  waiting for transfers between devices  191 us (65%)
  matrix products  34 us (12%)
  blocking collectives  23.4 us (8%)
  starting transfers between devices  15.8 us (5%)
  between operations  14 us (5%)
  local copies, waits for them, and re-layouts  7.02 us (2%)
  other arithmetic  6.89 us (2%)
    all_gather x1, waiting for transfers between devices, shards(): portion = lax.all_gather(arrived_rows, 'tp', axis=0, tiled=True)  60.5 us
    reduce_scatter x1, waiting for transfers between devices, shards(): lax.psum_scatter(jnp.dot(hidden, w_down, preferred_element_type=jnp.float...  58.9 us
    all_gather x1, waiting for transfers between devices, shards(): lax.all_gather(out_proj, 'tp', axis=0, tiled=True)  36.6 us
    all_gather x1, waiting for transfers between devices, shards(): lax.all_gather(normed, 'tp', axis=0, tiled=True)  33.5 us
    all_to_all x1, blocking collectives, shards(): lax.all_to_all(outgoing.reshape(experts, capacity, width_model), 'ep', sp...  23.4 us
    dot_general x1, matrix products, shards(): jnp.dot(hidden, w_down, preferred_element_type=jnp.float32)  14.9 us
    dot_general x1, matrix products, shards(): gate_value = jnp.dot(portion, w_gate, preferred_element_type=jnp.float32)  7.71 us
    all_to_all x1, starting transfers between devices, shards(): lax.all_to_all(summed.reshape(experts, capacity, width_model), 'ep', spli...  7.19 us
  transfers between devices with their start and end apart: 7, of which 5 were waited for; matrix products, arithmetic and copies ran while one was open for 13% of the time, Pallas kernels for 0%

commit v1 on v0

--- a/solution.py
+++ b/solution.py
@@ -1,9 +1,19 @@
+import functools
 import jax
 import jax.numpy as jnp
 from jax import lax
 from jax.sharding import PartitionSpec as P
 
 norm_eps = 1e-06
+
+
+def _plan_quarters(work_x, named_axis, along_dim):
+    left_arr = lax.all_to_all(jnp.stack(lax.axis_size(named_axis) * [work_x]), named_axis, 0, 0)
+    block_now = jnp.concatenate(left_arr, axis=along_dim)
+    return block_now
+
+
+test_shards = functools.partial(_plan_quarters, named_axis="tp", along_dim=0)
 
 
 def from_behind(value, axis, steps):
@@ -90,7 +100,7 @@
     w_gate = expert_gate[0]
     w_up = expert_up[0]
     w_down = expert_down[0]
-    portion = lax.all_gather(arrived_rows, "tp", axis=0, tiled=True)
+    portion = test_shards(arrived_rows)
     gate_value = jnp.dot(portion, w_gate, preferred_element_type=jnp.float32)
     up_value = jnp.dot(portion, w_up, preferred_element_type=jnp.float32)
     hidden = (jax.nn.silu(gate_value) * up_value).astype(jnp.bfloat16)

time: 293 us -> 452 us (1.54)
  waiting for transfers between devices: 191 us -> 335 us
  starting transfers between devices: 15.8 us -> 26.8 us
    all_to_all x0 -> x1, waiting for transfers between devices: none -> 244 us  [_plan_quarters(): lax.all_to_all(jnp.stack(lax.axis_size(named_axis) * [work_x]), named_axi...]
    all_gather x1 -> x0, waiting for transfers between devices: 60.5 us -> none  [shards(): portion = lax.all_gather(arrived_rows, 'tp', axis=0, tiled=True)]
    all_gather x1, waiting for transfers between devices: 33.5 us -> 0.02 us  [shards(): lax.all_gather(normed, 'tp', axis=0, tiled=True)]
    all_to_all x0 -> x1, starting transfers between devices: none -> 10.7 us  [_plan_quarters(): lax.all_to_all(jnp.stack(lax.axis_size(named_axis) * [work_x]), named_axi...]
    reduce_scatter x1, waiting for transfers between devices: 58.9 us -> 52.8 us  [shards(): lax.psum_scatter(jnp.dot(hidden, w_down, preferred_element_type=jnp.float...]
    another operation x0 -> x2, local copies, waits for them, and re-layouts: none -> 5.09 us  [_plan_quarters(): jnp.stack(lax.axis_size(named_axis) * [work_x])]
  transfers between devices with their start and end apart: 7 -> 7, of which waited for: 5 -> 4; matrix products, arithmetic and copies ran while one was open for 13% -> 8% of each run, Pallas kernels for 0% -> 0%
where the time goes in v1:
time: 452 us; the launch traced here: 451 us
  waiting for transfers between devices  335 us (74%)
  matrix products  34 us (8%)
  starting transfers between devices  26.8 us (6%)
  blocking collectives  23.4 us (5%)
  between operations  14 us (3%)
  local copies, waits for them, and re-layouts  11.3 us (2%)
  other arithmetic  6.92 us (2%)
    all_to_all x1, waiting for transfers between devices, _plan_quarters(): lax.all_to_all(jnp.stack(lax.axis_size(named_axis) * [work_x]), named_axi...  244 us
    reduce_scatter x1, waiting for transfers between devices, shards(): lax.psum_scatter(jnp.dot(hidden, w_down, preferred_element_type=jnp.float...  52.8 us
    all_gather x1, waiting for transfers between devices, shards(): lax.all_gather(out_proj, 'tp', axis=0, tiled=True)  36.9 us
    all_to_all x1, blocking collectives, shards(): lax.all_to_all(outgoing.reshape(experts, capacity, width_model), 'ep', sp...  23.4 us
    dot_general x1, matrix products, shards(): jnp.dot(hidden, w_down, preferred_element_type=jnp.float32)  14.9 us
    all_to_all x1, starting transfers between devices, _plan_quarters(): lax.all_to_all(jnp.stack(lax.axis_size(named_axis) * [work_x]), named_axi...  10.7 us
  transfers between devices with their start and end apart: 7, of which 4 were waited for; matrix products, arithmetic and copies ran while one was open for 8% of the time, Pallas kernels for 0%

profile of v1, /device:TPU:1, one launch (start us, length us, event | category | flops | bytes accessed | tf_op | source)
XLA Modules:
  0.0 451.2 jit_solution(4807373101079785079)
XLA Ops:
  7.2 0.9 copy.25
  8.0 0.1 eq.29
  8.2 0.1 fusion.24
  8.3 0.2 reduce_window_sum.11
  8.4 0.2 select_reduce_fusion
  8.6 0.1 reduce_sum.52
  8.8 0.1 copy.27
  8.9 0.1 fusion.23
  9.0 0.7 convert_element_type.89
  9.7 1.1 fusion.15
  10.8 1.3 convolution_convert_fusion.2
  12.1 0.2 reshape.89
  12.4 23.4 %all_to_all.34 = bf16[16,9,2048]{2,1,0:T(8,128)(2,1)S(1)} all-to-all(bf16[16,9,2048]{2,1,0:T(8,128)(2,1)S(1)} %reshape.89), channel_id=1, replica_groups=mesh['ep'=16,'tp'=16] {'ep'}, dimensions={0} | all-to-all | bytes 1179648 | tf_op jit(solution)/shard_map/all_to_all | solution.py:92
  35.8 0.3 stack_reshape.2
  36.0 4.8 %stack.3 = bf16[16,144,2048]{2,1,0:T(8,128)(2,1)} broadcast(bf16[144,2048]{1,0:T(8,128)(2,1)S(1)} %stack_reshape.2), dimensions={1,2} | broadcast | bytes 10027008 | tf_op jit(solution)/shard_map/stack | solution.py:11
  40.9 10.7 %all-to-all-start.2 = ((bf16[16,144,2048]{2,1,0:T(8,128)(2,1)}), bf16[16,144,2048]{2,1,0:T(8,128)(2,1)}, u32[]{:S(2)}, u32[]{:S(2)}) async-start(bf16[16,144,2048]{2,1,0:T(8,128)(2,1)} %stack.3), calls=%async_computation.2 | async-start | bytes 18874368 | tf_op jit(solution)/shard_map/all_to_all | solution.py:11
  51.5 0.0 all-gather.3.cloned.1.call-start
  51.6 0.2 fusion.2
  51.8 1.0 fusion.4
  52.8 0.0 reduce-scatter.2.cloned.1.call-start
  52.9 243.8 %all-to-all-done.2 = bf16[16,144,2048]{2,1,0:T(8,128)(2,1)} async-done(((bf16[16,144,2048]{2,1,0:T(8,128)(2,1)}), bf16[16,144,2048]{2,1,0:T(8,128)(2,1)}, u32[]{:S(2)}, u32[]{:S(2)}) %all-to-all-start.2) | async-done | bytes 9437216 | tf_op jit(solution)/shard_map/all_to_all | solution.py:11
  296.7 7.7 %fusion.8 = f32[2304,256]{1,0:T(8,128)} fusion(bf16[2304,2048]{1,0:T(8,128)(2,1)} %bitcast.5, bf16[1,2048,256]{2,1,0:T(8,128)(2,1)S(1)} %copy-done.5), kind=kOutput, calls=%fused_computation.15 | convolution fusion | flops 2415919104 | bytes 12845056 | tf_op jit(solution)/shard_map/dot_general | solution.py:104
  304.4 14.9 %convolution_convert_fusion = bf16[2304,2048]{1,0:T(8,128)(2,1)} fusion(bf16[2304,2048]{1,0:T(8,128)(2,1)} %bitcast.5, f32[2304,256]{1,0:T(8,128)} %fusion.8, bf16[1,256,2048]{2,1,0:T(8,128)(2,1)S(1)} %copy-done, bf16[1,2048,256]{2,1,0:T(8,128)(2,1)} %param.26), kind=kOutput, calls=%fused_computation.1 | convolution fusion | flops 4840095744 | bytes 23330816 | tf_op jit(solution)/shard_map/dot_general | solution.py:108
  319.3 0.0 reduce-scatter.2.cloned.1.call-update
  319.4 0.0 all-gather.5.cloned.1.call-start
  319.4 0.7 all-gather.5.cloned.1.call-update
  320.1 0.0 all-gather.3.cloned.1.call-done
  320.2 0.1 copy-done.6
  320.3 0.1 copy-done.7
  320.4 0.1 copy-done.8
  320.4 6.3 %convolution_convert_fusion.1 = bf16[2048,192]{0,1:T(8,128)(2,1)S(1)} fusion(bf16[2048,2048]{1,0:T(8,128)(2,1)} %all-gather.3.cloned.1.call-done, bf16[2048,64]{0,1:T(8,128)(2,1)S(1)} %copy-done.6, bf16[2048,64]{0,1:T(8,128)(2,1)S(1)} %copy-done.7, bf16[2048,64]{0,1:T(8,128)(2,1)S(1)} %copy-done.8), kind=kOutput, calls=%fused_computation.4 | convolution fusion | flops 1613365248 | bytes 9961472 | tf_op jit(solution)/shard_map/dot_general | solution.py:49
  326.7 0.1 multiply_convert_fusion.1
  326.8 0.1 slice.41
  326.9 2.4 collective-permute-start
  329.3 0.7 collective-permute-done
  329.9 1.0 copy_bitcast_fusion
  330.9 6.5 %all-to-all-start = ((bf16[16,128,64]{1,2,0:T(8,128)(2,1)}), bf16[16,128,64]{1,2,0:T(8,128)(2,1)S(1)}, u32[]{:S(2)}, u32[]{:S(2)}) async-start(bf16[16,128,64]{1,2,0:T(8,128)(2,1)} %copy_bitcast_fusion), calls=%async_computation | async-start | bytes 524288 | tf_op jit(solution)/shard_map/all_to_all | solution.py:70
  337.4 0.1 mul.138
  337.6 52.8 %reduce-scatter.2.cloned.1.call-done = bf16[144,2048]{1,0:T(8,128)(2,1)} async-done(((bf16[2304,2048]{1,0:T(8,128)(2,1)}), bf16[144,2048]{1,0:T(8,128)(2,1)}) %reduce-scatter.2.cloned.1.call-update) | async-done | bytes 589840 | tf_op jit(solution)/shard_map/reduce_scatter | solution.py:107
  390.4 2.3 reshape.91
  392.7 7.2 %all-to-all-start.3 = ((bf16[16,9,2048]{2,1,0:T(8,128)(2,1)}), bf16[16,9,2048]{2,1,0:T(8,128)(2,1)S(1)}, u32[]{:S(2)}, u32[]{:S(2)}) async-start(bf16[16,9,2048]{2,1,0:T(8,128)(2,1)} %reshape.91), calls=%async_computation.4 | async-start | bytes 2097152 | tf_op jit(solution)/shard_map/all_to_all | solution.py:113
  399.9 0.1 copy.24
  400.0 36.9 %all-gather.5.cloned.1.call-done = bf16[1024,2048]{1,0:T(8,128)(2,1)} async-done(((bf16[64,2048]{1,0:T(8,128)(2,1)}), bf16[1024,2048]{1,0:T(8,128)(2,1)}) %all-gather.5.cloned.1.call-update) | async-done | bytes 4194320 | tf_op jit(solution)/shard_map/all_gather | solution.py:73
  436.9 3.7 convolution_convert_fusion.3
  440.6 0.3 reshape.92
  440.9 0.9 gather_fusion
  441.8 0.7 reshape.93
  442.5 2.3 multiply_reduce_fusion
  (29 shorter events, 0.2 us)
Async XLA Ops:
  7.2 297.2 %copy-start = (bf16[1,256,2048]{2,1,0:T(8,128)(2,1)S(1)}, bf16[1,256,2048]{2,1,0:T(8,128)(2,1)}, u32[]{:S(2)}) copy-start(bf16[1,256,2048]{2,1,0:T(8,128)(2,1)} %param.27) | copy-start | bytes 3145732
  40.9 10.7 %copy-start.3 = (bf16[2048]{0:T(1024)(128)(2,1)S(1)}, bf16[2048]{0:T(1024)(128)(2,1)}, u32[]{:S(2)}) copy-start(bf16[2048]{0:T(1024)(128)(2,1)} %param.15) | copy-start | bytes 12292
  40.9 10.7 %copy-start.1 = (bf16[128,2048]{1,0:T(8,128)(2,1)S(1)}, bf16[128,2048]{1,0:T(8,128)(2,1)}, u32[]{:S(2)}) copy-start(bf16[128,2048]{1,0:T(8,128)(2,1)} %param.14) | copy-start | bytes 1572868
  40.9 255.8 %copy-start.5 = (bf16[1,2048,256]{2,1,0:T(8,128)(2,1)S(1)}, bf16[1,2048,256]{2,1,0:T(8,128)(2,1)}, u32[]{:S(2)}) copy-start(bf16[1,2048,256]{2,1,0:T(8,128)(2,1)} %param.25) | copy-start | bytes 3145732
  40.9 255.8 %all-to-all-start.2 = ((bf16[16,144,2048]{2,1,0:T(8,128)(2,1)}), bf16[16,144,2048]{2,1,0:T(8,128)(2,1)}, u32[]{:S(2)}, u32[]{:S(2)}) async-start(bf16[16,144,2048]{2,1,0:T(8,128)(2,1)} %stack.3), calls=%async_computation.2 | async-start | bytes 18874368 | tf_op jit(solution)/shard_map/all_to_all | solution.py:11
  51.5 268.6 %all-gather.3.cloned.1.call-start = ((), (), s32[]{:S(2)}) async-start(), calls=%async_computation.5 | async-start | bytes 8912896 | tf_op jit(solution)/shard_map/all_gather | solution.py:50
  52.8 337.6 %reduce-scatter.2.cloned.1.call-start = ((), (), s32[]{:S(2)}) async-start(), calls=%async_computation.7 | async-start | bytes 10027008 | tf_op jit(solution)/shard_map/reduce_scatter | solution.py:107
  319.3 0.8 copy-start.4
  319.3 1.0 copy-start.6
  319.3 1.0 copy-start.7
  319.3 1.1 copy-start.8
  319.4 117.5 %all-gather.5.cloned.1.call-start = ((), (), s32[]{:S(2)}) async-start(), calls=%async_computation.6 | async-start | bytes 4456448 | tf_op jit(solution)/shard_map/all_gather | solution.py:73
  320.1 17.4 %copy-start.2 = (f32[64,2]{0,1:T(2,128)S(1)}, f32[64,2]{0,1:T(2,128)}, u32[]{:S(2)}) copy-start(f32[64,2]{0,1:T(2,128)} %param.24) | copy-start | bytes 1540
  326.9 3.0 collective-permute-start
  330.9 61.8 %all-to-all-start = ((bf16[16,128,64]{1,2,0:T(8,128)(2,1)}), bf16[16,128,64]{1,2,0:T(8,128)(2,1)S(1)}, u32[]{:S(2)}, u32[]{:S(2)}) async-start(bf16[16,128,64]{1,2,0:T(8,128)(2,1)} %copy_bitcast_fusion), calls=%async_computation | async-start | bytes 524288 | tf_op jit(solution)/shard_map/all_to_all | solution.py:70
  392.7 47.9 %all-to-all-start.3 = ((bf16[16,9,2048]{2,1,0:T(8,128)(2,1)}), bf16[16,9,2048]{2,1,0:T(8,128)(2,1)S(1)}, u32[]{:S(2)}, u32[]{:S(2)}) async-start(bf16[16,9,2048]{2,1,0:T(8,128)(2,1)} %reshape.91), calls=%async_computation.4 | async-start | bytes 2097152 | tf_op jit(solution)/shard_map/all_to_all | solution.py:113
Sparse Core Ops, SparseCore 0:
  54.8 163.0 all-gather.2
  319.5 70.8 reduce-scatter.1
  392.2 44.5 all-gather.4
